TPU v7x, 32 devices: a whole 2x2x4 slice. The times are simulated.
32 devices in a mesh: ep: 8 (over z, core), tp: 4 (over y, x).
Axes of the slice: x: 2, y: 2, z: 4, core: 2. Of those that a mesh axis runs over, the one named last changes fastest.
Arguments:
- outer_gate: bfloat16 [1024, 2048], P('ep', 'tp'), may hold values from -6 to 6
- inner_gate: bfloat16 [1024, 2048], P('ep', 'tp'), may hold values from -6 to 6
- conv_value: bfloat16 [1024, 2048], P('ep', 'tp'), may hold values from -6 to 6
- conv_taps: bfloat16 [3, 2048], P(None, 'tp'), may hold values from -3.5 to 3.5
- mix_out: bfloat16 [2048, 2048], P(None, 'tp')
- gain_mixer: bfloat16 [2048], P('tp'), may hold values from 0.099609375 to 1.8984375
- bias_mixer: bfloat16 [2048], P('tp'), may hold values from -3 to 3
- moe_input: bfloat16 [1024, 2048], P('ep'), may hold values from -6 to 6
- route_ids: int32 [1024, 4], P('ep'), may hold values from 0 to 7, all different within a row; in each aligned block of 128 rows (0 to 127, 128 to 255, ...) at most 96 rows name the same one
- route_weights: float32 [1024, 4], P('ep'), may hold values from 0.1 to 1.2
- expert_gate: bfloat16 [8, 2048, 2048], P('ep', None, 'tp'), may hold values from -0.125 to 0.125
- expert_up: bfloat16 [8, 2048, 2048], P('ep', None, 'tp'), may hold values from -0.125 to 0.125
- expert_down: bfloat16 [8, 2048, 2048], P('ep', None, 'tp')
- shared_gate: bfloat16 [2048, 2048], P(None, 'tp'), may hold values from -0.125 to 0.125
- shared_up: bfloat16 [2048, 2048], P(None, 'tp'), may hold values from -0.125 to 0.125
- shared_down: bfloat16 [2048, 2048], P(None, 'tp')
- gain_experts: bfloat16 [2048], P('tp'), may hold values from 0.099609375 to 1.8984375
- bias_experts: bfloat16 [2048], P('tp'), may hold values from -3 to 3
Outputs:
- out_mixer: bfloat16 [1024, 2048], P('ep', 'tp')
- out_experts: bfloat16 [1024, 2048], P('ep', 'tp')
Inputs may be any that keep to these rules, and one draw needn't show every extreme that they name: `route_ids`: each row names 4 different experts. Among the rows of one index of ep (aligned blocks of 128 rows) no expert is named more than 96 times, a bound that some block reaches.
All inputs are finite; a program needn't handle non-finite values.
Results may differ from a plain program's by a relative error of at most 0.0055.
Values may be sent and summed in bfloat16 or wider, within the bound.
A program may use at most 64 MiB of HBM per device.

v0:
```python
import jax
import jax.numpy as jnp
from jax import lax
from jax.sharding import PartitionSpec as P

SEQS = 1


def shifted(block, axis, distance):
    devices = range(lax.axis_size(axis))
    route = [(i - distance, i) for i in devices if i - distance in devices]
    return lax.ppermute(block, axis, route)


def finish(values, totals, squares, full_width, gain, offset_bias):
    average = (totals / full_width)[:, None]
    spread = (squares / full_width)[:, None] - average * average
    scaled = (values - average) * lax.rsqrt(spread + 1e-05)
    return (scaled * gain.astype(jnp.float32) + offset_bias.astype(jnp.float32)).astype(
        jnp.bfloat16
    )


def on_device(
    outer_gate,
    inner_gate,
    conv_value,
    conv_taps,
    mix_out,
    gain_mixer,
    bias_mixer,
    moe_input,
    route_ids,
    route_weights,
    expert_gate,
    expert_up,
    expert_down,
    shared_gate,
    shared_up,
    shared_down,
    gain_experts,
    bias_experts,
):
    token_rows = outer_gate.shape[0]
    column_count = outer_gate.shape[1]
    ep_count = lax.axis_size("ep")
    tp_count = lax.axis_size("tp")
    taps_count = conv_taps.shape[0]
    product = (inner_gate.astype(jnp.float32) * conv_value.astype(jnp.float32)).astype(jnp.bfloat16)
    border = shifted(product[token_rows - (taps_count - 1) :], "ep", 1)
    extended = jnp.concatenate([border, product], axis=0).astype(jnp.float32)
    seq_length = token_rows * ep_count // SEQS
    places = (
        lax.axis_index("ep") * token_rows + jnp.arange(token_rows, dtype=jnp.int32)
    ) % seq_length
    convolved = jnp.zeros((token_rows, column_count), jnp.float32)
    for offset in range(taps_count):
        delay_rows = taps_count - 1 - offset
        delayed = extended[offset : offset + token_rows]
        kept_mask = (places >= delay_rows).astype(jnp.float32)[:, None]
        convolved = convolved + conv_taps[offset].astype(jnp.float32)[None, :] * delayed * kept_mask
    weighted_in = (outer_gate.astype(jnp.float32) * convolved).astype(jnp.bfloat16)
    block = mix_out
    mixed = jnp.dot(
        lax.all_gather(weighted_in, "tp", axis=1, tiled=True),
        block,
        preferred_element_type=jnp.float32,
    )
    topk_count = route_ids.shape[1]
    local_experts = expert_gate.shape[0]
    expert_count = local_experts * ep_count
    capacity = max(2, 3 * token_rows * topk_count // (2 * expert_count))
    flat_ids = route_ids.reshape(-1)
    marks = (flat_ids[:, None] == jnp.arange(expert_count, dtype=jnp.int32)[None, :]).astype(
        jnp.int32
    )
    ranks = jnp.sum((jnp.cumsum(marks, axis=0) - marks) * marks, axis=1)
    targets = flat_ids * capacity + ranks
    sources = jnp.arange(flat_ids.shape[0], dtype=jnp.int32) // topk_count
    sent_rows = lax.dynamic_slice_in_dim(
        moe_input, lax.axis_index("tp") * column_count, column_count, 1
    )
    buffer_rows = jnp.zeros((expert_count * capacity, sent_rows.shape[1]), jnp.bfloat16)
    buffer_rows = buffer_rows.at[targets].set(sent_rows[sources])
    sectioned = buffer_rows.reshape(ep_count, local_experts * capacity, sent_rows.shape[1])
    arrived = lax.all_to_all(sectioned, "ep", split_axis=0, concat_axis=0, tiled=True)
    arrived = lax.all_gather(arrived, "tp", axis=2, tiled=True)
    expert_rows = arrived.reshape(ep_count, local_experts, capacity, arrived.shape[2])
    gate_value = jnp.einsum(
        "secd,edf->secf", expert_rows, expert_gate, preferred_element_type=jnp.float32
    )
    up_value = jnp.einsum(
        "secd,edf->secf", expert_rows, expert_up, preferred_element_type=jnp.float32
    )
    hidden = (jax.nn.silu(gate_value) * up_value).astype(jnp.bfloat16)
    flat_hidden = hidden.reshape(expert_count * capacity, hidden.shape[3])
    shared_gate_value = jnp.dot(moe_input, shared_gate, preferred_element_type=jnp.float32)
    shared_up_value = jnp.dot(moe_input, shared_up, preferred_element_type=jnp.float32)
    shared_hidden = (jax.nn.silu(shared_gate_value) * shared_up_value).astype(jnp.bfloat16)
    piece = lax.all_gather(flat_hidden, "tp", axis=1, tiled=True)
    block = expert_down
    shaped = piece.reshape(ep_count, local_experts, capacity, piece.shape[1])
    routed_sum = jnp.einsum("secf,efd->secd", shaped, block, preferred_element_type=jnp.float32)
    block = shared_down
    shared_sum = jnp.dot(
        lax.all_gather(shared_hidden, "tp", axis=1, tiled=True),
        block,
        preferred_element_type=jnp.float32,
    )
    expert_out = routed_sum.astype(jnp.bfloat16).reshape(
        ep_count, local_experts * capacity, column_count
    )
    returned = lax.all_to_all(expert_out, "ep", split_axis=0, concat_axis=0, tiled=True)
    picked = returned.reshape(expert_count * capacity, column_count)[targets].astype(jnp.float32)
    weighted = picked.reshape(token_rows, topk_count, column_count) * route_weights[:, :, None]
    combined = jnp.sum(weighted, axis=1) + shared_sum
    mixer_total, mixer_square, expert_total, expert_square = lax.psum(
        (
            jnp.sum(mixed, axis=1),
            jnp.sum(mixed * mixed, axis=1),
            jnp.sum(combined, axis=1),
            jnp.sum(combined * combined, axis=1),
        ),
        "tp",
    )
    full_width = column_count * tp_count
    out_mixer = finish(mixed, mixer_total, mixer_square, full_width, gain_mixer, bias_mixer)
    out_experts = finish(
        combined, expert_total, expert_square, full_width, gain_experts, bias_experts
    )
    return (out_mixer, out_experts)


def solution(mesh):
    in_specs = (
        P("ep", "tp"),
        P("ep", "tp"),
        P("ep", "tp"),
        P(None, "tp"),
        P(None, "tp"),
        P("tp"),
        P("tp"),
        P("ep", None),
        P("ep", None),
        P("ep", None),
        P("ep", None, "tp"),
        P("ep", None, "tp"),
        P("ep", None, "tp"),
        P(None, "tp"),
        P(None, "tp"),
        P(None, "tp"),
        P("tp"),
        P("tp"),
    )
    out_specs = (P("ep", "tp"), P("ep", "tp"))
    return jax.shard_map(
        on_device, mesh=mesh, in_specs=in_specs, out_specs=out_specs, check_vma=False
    )
```

profile of v0, /device:TPU:0, one launch (start us, length us, event | category | flops | bytes accessed | tf_op | source)
XLA Modules:
  0.0 202.3 jit_solution(16404926073839543372)
XLA Ops:
  7.2 0.9 copy.22
  8.4 0.7 broadcast_multiply_fusion
  9.1 1.1 reduce-window.6
  10.7 0.9 constant_dynamic-slice_fusion
  11.8 4.9 %scatter_custom_fusion = bf16[768,512]{1,0:T(8,128)(2,1)S(1)} fusion(s32[512]{0:T(512)S(1)} %bitcast.76, bf16[128,512]{1,0:T(8,128)(2,1)S(1)} %constant_dynamic-slice_fusion, s32[1024]{0:T(1024)S(1)} %pad_clamp_fusion.1, bf16[]{:T(256)} %constant.69.clone.1), kind=kCustom, calls=%fused_computation.21 | custom fusion | bytes 786434 | tf_op jit(solution)/shard_map/scatter | solution.py:84
  16.7 27.2 %all_to_all.10 = bf16[8,96,512]{2,1,0:T(8,128)(2,1)} all-to-all(bf16[8,96,512]{2,1,0:T(8,128)(2,1)S(1)} %bitcast.71), channel_id=1, replica_groups=mesh['ep'=8,'tp'=4] {'ep'}, dimensions={0} | all-to-all | bytes 1572864 | tf_op jit(solution)/shard_map/all_to_all | solution.py:86
  44.0 42.8 %all-gather.3.cloned.1.call-done = bf16[8,96,2048]{2,1,0:T(8,128)(2,1)} async-done(((bf16[8,96,512]{2,1,0:T(8,128)(2,1)}), bf16[8,96,2048]{2,1,0:T(8,128)(2,1)}) %all-gather.3.cloned.1.call-update) | async-done | bytes 3145744 | tf_op jit(solution)/shard_map/all_gather | solution.py:87
  86.7 3.8 %fusion.4 = f32[8,96,512]{2,1,0:T(8,128)S(1)} fusion(bf16[8,96,2048]{2,1,0:T(8,128)(2,1)} %all-gather.3.cloned.1.call-done, bf16[1,2048,512]{2,1,0:T(8,128)(2,1)S(1)} %copy-done), kind=kOutput, calls=%fused_computation.7 | convolution fusion | flops 1610612736 | bytes 6815744 | tf_op jit(solution)/shard_map/secd,edf->secf/dot_general | solution.py:89
  90.6 2.8 %fusion.6 = bf16[8,1,96,512]{3,2,0,1:T(8,128)(2,1)} fusion(f32[8,96,512]{2,1,0:T(8,128)S(1)} %fusion.4, bf16[8,96,2048]{2,1,0:T(8,128)(2,1)S(1)} %copy-done.10, bf16[1,2048,512]{2,1,0:T(8,128)(2,1)S(1)} %copy-done.11), kind=kOutput, calls=%fused_computation.10 | convolution fusion | flops 1612972032 | bytes 7602176 | tf_op jit(solution)/shard_map/secd,edf->secf/dot_general | solution.py:92
  94.1 2.1 %collective-permute-start = (bf16[2,512]{1,0:T(2,128)(2,1)}, bf16[2,512]{1,0:T(2,128)(2,1)}, u32[]{:S(2)}, u32[]{:S(2)}) collective-permute-start(bf16[2,512]{1,0:T(2,128)(2,1)} %slice.40), channel_id=1, source_target_pairs={{0,4},{4,8},{8,12},{12,16},{16,20},{20,24},{24,28},{1,5},{5,9},{9,... | collective-permute-start | bytes 6152 | tf_op jit(solution)/shard_map/ppermute | solution.py:12
  96.3 0.6 compare_convert_fusion
  96.9 2.8 %fusion.32 = f32[128,512]{1,0:T(8,128)} fusion(bf16[128,2048]{1,0:T(8,128)(2,1)S(1)} %copy-done.2, bf16[2048,512]{1,0:T(8,128)(2,1)} %param.31), kind=kOutput, calls=%fused_computation.73 | convolution fusion | flops 268435456 | bytes 2883584 | tf_op jit(solution)/shard_map/dot_general | solution.py:97
  99.6 37.7 %all-gather.5.cloned.1.call-done = bf16[768,2048]{1,0:T(8,128)(2,1)} async-done(((bf16[768,512]{1,0:T(8,128)(2,1)}), bf16[768,2048]{1,0:T(8,128)(2,1)}) %all-gather.5.cloned.1.call-update) | async-done | bytes 3145744 | tf_op jit(solution)/shard_map/all_gather | solution.py:100
  137.4 5.2 %fusion.12 = bf16[8,96,512]{2,1,0:T(8,128)(2,1)} fusion(bf16[8,96,2048]{2,1,0:T(8,128)(2,1)} %bitcast.80, bf16[1,2048,512]{2,1,0:T(8,128)(2,1)} %param.30), kind=kOutput, calls=%fused_computation.16 | convolution fusion | flops 1611005952 | bytes 6029312 | tf_op jit(solution)/shard_map/secf,efd->secd/dot_general | solution.py:103
  142.6 4.6 %all-to-all-start.1 = ((bf16[8,96,512]{2,1,0:T(8,128)(2,1)}), bf16[8,96,512]{2,1,0:T(8,128)(2,1)S(1)}, u32[]{:S(2)}, u32[]{:S(2)}) async-start(bf16[8,96,512]{2,1,0:T(8,128)(2,1)} %fusion.12), calls=%async_computation.1 | async-start | bytes 1572864 | tf_op jit(solution)/shard_map/all_to_all | solution.py:113
  147.8 0.6 slice_convert_fusion.2
  148.4 2.1 %fusion.15 = bf16[128,512]{1,0:T(8,128)(2,1)S(1)} fusion(bf16[128,2048]{1,0:T(8,128)(2,1)S(1)} %copy-done.2, bf16[2048,512]{1,0:T(8,128)(2,1)} %param.32, f32[128,512]{1,0:T(8,128)} %fusion.32), kind=kOutput, calls=%fused_computation.19 | convolution fusion | flops 268828672 | bytes 3014656 | tf_op jit(solution)/shard_map/dot_general | solution.py:98
  150.4 11.2 %all_gather.15 = bf16[128,2048]{1,0:T(8,128)(2,1)} all-gather(bf16[128,512]{1,0:T(8,128)(2,1)S(1)} %fusion.15), channel_id=1, replica_groups=mesh['ep'=8,'tp'=4] {'tp'}, dimensions={1}, use_global_device_ids=true | all-gather | bytes 655360 | tf_op jit(solution)/shard_map/all_gather | solution.py:106
  161.6 0.7 copy.24
  162.4 1.4 convert_element_type.109
  163.8 0.7 convert_element_type.98
  164.5 0.7 convert_element_type.99
  165.1 0.7 maximum_convert_fusion
  165.9 1.1 fusion.22
  166.9 10.4 %all_gather.12 = bf16[128,2048]{1,0:T(8,128)(2,1)S(1)} all-gather(bf16[128,512]{1,0:T(8,128)(2,1)S(1)} %fusion.22), channel_id=1, replica_groups=mesh['ep'=8,'tp'=4] {'tp'}, dimensions={1}, use_global_device_ids=true | all-gather | bytes 655360 | tf_op jit(solution)/shard_map/all_gather | solution.py:65
  177.9 2.6 %gather_fusion = bf16[512,512]{1,0:T(8,128)(2,1)} fusion(bf16[768,512]{1,0:T(8,128)(2,1)S(1)} %bitcast.70, s32[1024]{0:T(1024)S(1)} %pad_clamp_fusion), kind=kCustom, calls=%fused_computation.1 | custom fusion | bytes 1050624 | tf_op jit(solution)/shard_map/gather | solution.py:114
  180.5 1.4 reshape.183
  181.9 0.7 multiply_reduce_fusion
  182.6 2.3 %fusion.30 = (f32[128]{0:T(128)S(1)}, f32[128]{0:T(128)S(1)}, f32[128,512]{1,0:T(8,128)S(1)}) fusion(f32[128,512]{1,0:T(8,128)S(1)} %multiply_reduce_fusion, bf16[128,2048]{1,0:T(8,128)(2,1)} %all_gather.15, bf16[2048,512]{1,0:T(8,128)(2,1)} %param.33), kind=kOutput, calls=%fused_computation.71 | convolution fusion | flops 268697344 | bytes 3146752 | tf_op jit(solution)/shard_map/dot_general | solution.py:105
  184.9 8.9 %all-reduce = (f32[128]{0:T(128)S(1)}, f32[128]{0:T(128)S(1)}, f32[128]{0:T(128)S(1)}, f32[128]{0:T(128)S(1)}) all-reduce(f32[128]{0:T(128)S(1)} %get-tuple-element.5, f32[128]{0:T(128)S(1)} %get-tuple-element.4, f32[128]{0:T(128)S(1)} %get-tuple-element.3, f32[128]{0:T(128)S(1)} %get-tuple-element.2), channel_id=1, replica_groups=mesh['ep'=8,'tp'=4] {'tp'}, use_global_device_ids=true, to_apply=%region_3.4 | all-reduce | flops 512 | bytes 4096 | tf_op jit(solution)/shard_map/psum | solution.py:117
  193.9 0.8 add_convert_fusion
  194.7 0.8 add_convert_fusion.1
  (50 shorter events, 2.7 us)
Async XLA Ops:
  7.2 79.6 %copy-start = (bf16[1,2048,512]{2,1,0:T(8,128)(2,1)S(1)}, bf16[1,2048,512]{2,1,0:T(8,128)(2,1)}, u32[]{:S(2)}) copy-start(bf16[1,2048,512]{2,1,0:T(8,128)(2,1)} %param.28) | copy-start | bytes 6291460
  7.2 79.6 %all-gather.3.cloned.1.call-start = ((), (), s32[]{:S(2)}) async-start(), calls=%async_computation.2 | async-start | bytes 3932160 | tf_op jit(solution)/shard_map/all_gather | solution.py:87
  43.9 93.4 %all-gather.5.cloned.1.call-start = ((), (), s32[]{:S(2)}) async-start(), calls=%async_computation.3 | async-start | bytes 3932160 | tf_op jit(solution)/shard_map/all_gather | solution.py:100
  86.7 3.8 %copy-start.10 = (bf16[8,96,2048]{2,1,0:T(8,128)(2,1)S(1)}, bf16[8,96,2048]{2,1,0:T(8,128)(2,1)}, u32[]{:S(2)}) copy-start(bf16[8,96,2048]{2,1,0:T(8,128)(2,1)} %all-gather.3.cloned.1.call-done) | copy-start | bytes 9437188
  86.7 3.8 %copy-start.11 = (bf16[1,2048,512]{2,1,0:T(8,128)(2,1)S(1)}, bf16[1,2048,512]{2,1,0:T(8,128)(2,1)}, u32[]{:S(2)}) copy-start(bf16[1,2048,512]{2,1,0:T(8,128)(2,1)} %param.29) | copy-start | bytes 6291460
  90.6 2.9 %copy-start.4 = (bf16[128,512]{1,0:T(8,128)(2,1)S(1)}, bf16[128,512]{1,0:T(8,128)(2,1)}, u32[]{:S(2)}) copy-start(bf16[128,512]{1,0:T(8,128)(2,1)} %param.20) | copy-start | bytes 393220
  90.6 2.9 %copy-start.5 = (bf16[128,512]{1,0:T(8,128)(2,1)S(1)}, bf16[128,512]{1,0:T(8,128)(2,1)}, u32[]{:S(2)}) copy-start(bf16[128,512]{1,0:T(8,128)(2,1)} %param.19) | copy-start | bytes 393220
  90.6 6.3 %copy-start.2 = (bf16[128,2048]{1,0:T(8,128)(2,1)S(1)}, bf16[128,2048]{1,0:T(8,128)(2,1)}, u32[]{:S(2)}) copy-start(bf16[128,2048]{1,0:T(8,128)(2,1)} %param.25) | copy-start | bytes 1572868
  94.1 71.0 %collective-permute-start = (bf16[2,512]{1,0:T(2,128)(2,1)}, bf16[2,512]{1,0:T(2,128)(2,1)}, u32[]{:S(2)}, u32[]{:S(2)}) collective-permute-start(bf16[2,512]{1,0:T(2,128)(2,1)} %slice.40), channel_id=1, source_target_pairs={{0,4},{4,8},{8,12},{12,16},{16,20},{20,24},{24,28},{1,5},{5,9},{9,... | collective-permute-start | bytes 6152 | tf_op jit(solution)/shard_map/ppermute | solution.py:12
  137.4 10.4 %copy-start.6 = (bf16[3,512]{1,0:T(4,128)(2,1)S(1)}, bf16[3,512]{1,0:T(4,128)(2,1)}, u32[]{:S(2)}) copy-start(bf16[3,512]{1,0:T(4,128)(2,1)} %param.21) | copy-start | bytes 9220
  142.6 35.3 %all-to-all-start.1 = ((bf16[8,96,512]{2,1,0:T(8,128)(2,1)}), bf16[8,96,512]{2,1,0:T(8,128)(2,1)S(1)}, u32[]{:S(2)}, u32[]{:S(2)}) async-start(bf16[8,96,512]{2,1,0:T(8,128)(2,1)} %fusion.12), calls=%async_computation.1 | async-start | bytes 1572864 | tf_op jit(solution)/shard_map/all_to_all | solution.py:113
  147.2 14.4 %copy-start.8 = (f32[128,4]{0,1:T(4,128)S(1)}, f32[128,4]{0,1:T(4,128)}, u32[]{:S(2)}) copy-start(f32[128,4]{0,1:T(4,128)} %param.27) | copy-start | bytes 6148
  148.4 14.0 %copy-start.9 = (bf16[512]{0:T(512)(128)(2,1)S(1)}, bf16[512]{0:T(512)(128)(2,1)}, u32[]{:S(2)}) copy-start(bf16[512]{0:T(512)(128)(2,1)} %param.34) | copy-start | bytes 3076
  162.4 14.9 %copy-start.1 = (bf16[2048,512]{1,0:T(8,128)(2,1)S(1)}, bf16[2048,512]{1,0:T(8,128)(2,1)}, u32[]{:S(2)}) copy-start(bf16[2048,512]{1,0:T(8,128)(2,1)} %param.22) | copy-start | bytes 6291460
  177.9 4.0 %copy-start.3 = (f32[128,4]{1,0:T(8,128)S(1)}, f32[128,4]{1,0:T(8,128)}, u32[]{:S(2)}) copy-start(f32[128,4]{1,0:T(8,128)} %copy.24) | copy-start | bytes 6148
  181.9 12.0 %copy-start.7 = (f32[512]{0:T(512)S(1)}, f32[512]{0:T(512)}, u32[]{:S(2)}) copy-start(f32[512]{0:T(512)} %convert_element_type.109) | copy-start | bytes 6148
Sparse Core Ops, SparseCore 0:
  44.1 42.6 all-gather.2
  93.6 43.7 all-gather.4
where the time goes:
time: 203 us; the launch traced here: 202 us
  waiting for transfers between devices  80.5 us (40%)
  blocking collectives  57.7 us (28%)
  matrix products  19.5 us (10%)
  between operations  14.3 us (7%)
  local copies, waits for them, and re-layouts  12.8 us (6%)
  other arithmetic  10.6 us (5%)
  starting transfers between devices  6.82 us (3%)
    all_gather x1, waiting for transfers between devices, on_device(): arrived = lax.all_gather(arrived, 'tp', axis=2, tiled=True)  42.8 us
    all_gather x1, waiting for transfers between devices, on_device(): piece = lax.all_gather(flat_hidden, 'tp', axis=1, tiled=True)  37.7 us
    all_to_all x1, blocking collectives, on_device(): lax.all_to_all(sectioned, 'ep', split_axis=0, concat_axis=0, tiled=True)  27.2 us
    all_gather x1, blocking collectives, on_device(): lax.all_gather(shared_hidden, 'tp', axis=1, tiled=True)  11.2 us
    all_gather x1, blocking collectives, on_device(): lax.all_gather(weighted_in, 'tp', axis=1, tiled=True)  10.4 us
    psum x1, blocking collectives, on_device(): lax.psum((jnp.sum(mixed, axis=1), jnp.sum(mixed * mixed, axis=1), jnp.sum...  8.95 us
    dot_general x1, matrix products, on_device(): jnp.einsum('secf,efd->secd', shaped, block, preferred_element_type=jnp.fl...  5.22 us
    scatter x1, local copies, waits for them, and re-layouts, on_device(): buffer_rows = buffer_rows.at[targets].set(sent_rows[sources])  4.94 us
  transfers between devices with their start and end apart: 4, of which 2 were waited for; matrix products, arithmetic and copies ran while one was open for 9% of the time, Pallas kernels for 0%

commit v1 on v0

--- a/solution.py
+++ b/solution.py
@@ -1,6 +1,10 @@
+import functools
+
 import jax
 import jax.numpy as jnp
 from jax import lax
+from jax.experimental import pallas as pl
+from jax.experimental.pallas import tpu as pltpu
 from jax.sharding import PartitionSpec as P
 
 SEQS = 1
@@ -21,7 +25,7 @@
     )
 
 
-def on_device(
+def plain_device(
     outer_gate,
     inner_gate,
     conv_value,
@@ -131,6 +135,427 @@
     return (out_mixer, out_experts)
 
 
+PLANE = 2
+CORES = 2
+VMEM_BYTES = 60 * 1024 * 1024
+
+
+def silu(value):
+    return value / (1.0 + jnp.exp(-value))
+
+
+def fused_kernel(
+    shape,
+    outer_ref,
+    inner_ref,
+    value_ref,
+    taps_ref,
+    mix_hbm,
+    gain_m_ref,
+    bias_m_ref,
+    moe_ref,
+    weights_ref,
+    gate_hbm,
+    up_hbm,
+    down_hbm,
+    shared_gate_hbm,
+    shared_up_hbm,
+    shared_down_hbm,
+    gain_e_ref,
+    bias_e_ref,
+    out_m_ref,
+    out_e_ref,
+    mix_v,
+    gate_v,
+    up_v,
+    down_v,
+    shared_gate_v,
+    shared_up_v,
+    shared_down_v,
+    tokens,
+    route,
+    rows_in,
+    hidden,
+    weighted,
+    shared_hidden,
+    border,
+    edge,
+    extended,
+    peer_part,
+    own_part,
+    sent_sum,
+    returned,
+    stats_out,
+    stats_in,
+    mixed_ref,
+    total_ref,
+    load_sem,
+    send_sem,
+    recv_sem,
+):
+    ep_count, tp_count, capacity, seq_length = shape
+    chips = ep_count // CORES
+    rows, cols = outer_ref.shape
+    full_width = cols * tp_count
+    me = lax.axis_index("ep")
+    j = lax.axis_index("tp")
+    z = me // CORES
+    c = me % CORES
+    x = j % PLANE
+    y = j // PLANE
+    jx = y * PLANE + (1 - x)
+    jy = (1 - y) * PLANE + x
+    jd = (1 - y) * PLANE + (1 - x)
+    other = z * CORES + (1 - c)
+    f32, bf16 = jnp.float32, jnp.bfloat16
+
+    order = (
+        (shared_gate_hbm, shared_gate_v),
+        (shared_up_hbm, shared_up_v),
+        (gate_hbm.at[0], gate_v),
+        (up_hbm.at[0], up_v),
+        (mix_hbm, mix_v),
+        (down_hbm.at[0], down_v),
+        (shared_down_hbm, shared_down_v),
+    )
+    loads = [pltpu.make_async_copy(a, b, load_sem.at[n]) for n, (a, b) in enumerate(order)]
+    for load in loads:
+        load.start()
+
+    product = (inner_ref[...].astype(f32) * value_ref[...].astype(f32)).astype(bf16)
+    edge_rows = edge.shape[0]
+    edge[...] = product[rows - edge_rows :]
+    pad = extended.shape[0] - rows
+    extended[pad:, :] = product.astype(f32)
+    route[0, 0] = weights_ref[...]
+
+    barrier = pltpu.get_barrier_semaphore()
+    for step in range(1, ep_count):
+        pl.semaphore_signal(barrier, inc=1, device_id=((me + step) % ep_count, j), device_id_type=pl.DeviceIdType.MESH)
+    for peer in (jx, jy, jd):
+        pl.semaphore_signal(barrier, inc=1, device_id=(me, peer), device_id_type=pl.DeviceIdType.MESH)
+    pl.semaphore_wait(barrier, ep_count - 1 + tp_count - 1)
+
+    numbers = {}
+    started = []
+
+    def number(name):
+        return numbers.setdefault(name, len(numbers))
+
+    def copy(name, source, target, device):
+        n = number(name)
+        return pltpu.make_async_remote_copy(
+            src_ref=source,
+            dst_ref=target,
+            send_sem=send_sem.at[n],
+            recv_sem=recv_sem.at[n],
+            device_id=device,
+            device_id_type=pl.DeviceIdType.MESH,
+        )
+
+    def send(name, source, target, device):
+        c_ = copy(name, source, target, device)
+        c_.start()
+        started.append(c_)
+
+    def arrive(name, target):
+        copy(name, target, target, (other, j)).wait_recv()
+
+    def columns(owner):
+        return pl.ds(pl.multiple_of(owner * cols, cols), cols)
+
+    def gather_start(name, ref):
+        part = ref.at[:, columns(j)]
+        send(name + ("x",), part, part, (me, jx))
+        send(name + ("y",), part, part, (me, jy))
+
+    def gather_relay(name, ref):
+        half = ref.shape[0] // 2
+        arrive(name + ("x",), ref.at[:, columns(jx)])
+        part = ref.at[pl.ds(0, half), columns(jx)]
+        send(name + ("xy",), part, part, (me, jy))
+        arrive(name + ("y",), ref.at[:, columns(jy)])
+        part = ref.at[pl.ds(half, half), columns(jy)]
+        send(name + ("yx",), part, part, (me, jx))
+
+    def gather_finish(name, ref):
+        half = ref.shape[0] // 2
+        arrive(name + ("xy",), ref.at[pl.ds(0, half), columns(jd)])
+        arrive(name + ("yx",), ref.at[pl.ds(half, half), columns(jd)])
+
+    send(("pair", 0), moe_ref, tokens.at[0, 1], (other, j))
+    for s in range(chips):
+        target = (z - s + chips) % chips
+        if s > 0:
+            send(("route", s, 0), weights_ref, route.at[s, 0], (target * CORES + c, j))
+        send(("route", s, 1), weights_ref, route.at[s, 1], (target * CORES + (1 - c), j))
+    for s in range(1, chips):
+        target = (z - s + chips) % chips
+        send(
+            ("line", s),
+            moe_ref.at[:, columns(j)],
+            tokens.at[s, 0, :, columns(j)],
+            (target * CORES + c, j),
+        )
+    send(("edge",), edge, border, ((me + 1) % ep_count, j))
+
+    def dot(a, b):
+        return jnp.dot(a, b, preferred_element_type=f32)
+
+    loads[0].wait()
+    loads[1].wait()
+    held = silu(dot(moe_ref[...], shared_gate_v[...])) * dot(moe_ref[...], shared_up_v[...])
+    shared_hidden[:, columns(j)] = held.astype(bf16)
+    gather_start(("shared",), shared_hidden)
+
+    arrive(("edge",), border)
+    extended[pad - edge_rows : pad, :] = border[...].astype(f32)
+    places = (me * rows + lax.broadcasted_iota(jnp.int32, (rows, 1), 0)) % seq_length
+    taps_count = taps_ref.shape[0]
+    convolved = jnp.zeros((rows, cols), f32)
+    for offset in range(taps_count):
+        delay = taps_count - 1 - offset
+        delayed = extended[pad - delay : pad - delay + rows, :]
+        kept = (places >= delay).astype(f32)
+        convolved = convolved + taps_ref[offset : offset + 1, :].astype(f32) * delayed * kept
+    weighted[:, columns(j)] = (outer_ref[...].astype(f32) * convolved).astype(bf16)
+    gather_start(("mixer",), weighted)
+
+    def token_ref(s, p):
+        return moe_ref if (s, p) == (0, 0) else tokens.at[s, p]
+
+    def choice(s, p):
+        weight = route[s, p, pl.ds(me, 1), :]
+        routed = (weight > 0.0).astype(f32)
+        earlier = lax.broadcasted_iota(jnp.int32, (rows, rows), 0)
+        later = lax.broadcasted_iota(jnp.int32, (rows, rows), 1)
+        upper = (earlier <= later).astype(f32).astype(bf16)
+        many = jnp.broadcast_to(routed, (16, rows)).astype(bf16)
+        rank = dot(many, upper)[0:1, :] * routed
+        slot = lax.broadcasted_iota(jnp.int32, (capacity, rows), 0).astype(f32) + 1.0
+        return (slot == rank).astype(f32), weight
+
+    def expert_up_stage(s):
+        for p in range(CORES):
+            picks, _ = choice(s, p)
+            rows_in[p * capacity : (p + 1) * capacity, :] = dot(
+                picks.astype(bf16), token_ref(s, p)[...]
+            ).astype(bf16)
+        held = silu(dot(rows_in[...], gate_v[...])) * dot(rows_in[...], up_v[...])
+        hidden[s, :, columns(j)] = held.astype(bf16)
+        gather_start(("hidden", s), hidden.at[s])
+
+    def expert_down_stage(s):
+        full = dot(hidden[s], down_v[...])
+        for p in reversed(range(CORES)):
+            picks, weight = choice(s, p)
+            scale = jnp.sum(picks * weight, axis=1, keepdims=True)
+            scaled = (full[p * capacity : (p + 1) * capacity] * scale).astype(bf16)
+            spread = lax.dot_general(
+                picks.astype(bf16), scaled, (((0,), (0,)), ((), ())), preferred_element_type=f32
+            )
+            if p == 1:
+                own_part[s] = spread.astype(bf16)
+                send(("part", s), own_part.at[s], peer_part.at[s], (other, j))
+            elif s == 0:
+                total_ref[...] = spread
+            else:
+                sent_sum[s] = spread.astype(bf16)
+
+    def expert_return(s):
+        arrive(("part", s), peer_part.at[s])
+        if s == 0:
+            total_ref[...] = total_ref[...] + peer_part[0].astype(f32)
+        else:
+            sent_sum[s] = (sent_sum[s].astype(f32) + peer_part[s].astype(f32)).astype(bf16)
+            target = (z + s) % chips
+            send(("return", s), sent_sum.at[s], returned.at[s], (target * CORES + c, j))
+
+    def wait_routes(s):
+        for p in range(CORES):
+            if (s, p) != (0, 0):
+                arrive(("route", s, p), route.at[s, p])
+
+    def pair_tokens(s):
+        gather_finish(("tokens", s), tokens.at[s, 0])
+        send(("pair", s), tokens.at[s, 0], tokens.at[s, 1], (other, j))
+
+    def line_tokens(s):
+        arrive(("line", s), tokens.at[s, 0, :, columns(j)])
+        gather_start(("tokens", s), tokens.at[s, 0])
+
+    def stats_start(k, values):
+        lane = lax.broadcasted_iota(jnp.int32, (rows, rows), 1)
+        total = jnp.sum(values, axis=1, keepdims=True)
+        square = jnp.sum(values * values, axis=1, keepdims=True)
+        tile = jnp.where(lane == 0, total, jnp.where(lane == 1, square, 0.0))
+        stats_out[k] = tile.T[0 : stats_out.shape[1], :]
+        for n, peer in enumerate((jx, jy, jd)):
+            send(("stats", k, n), stats_out.at[k], stats_in.at[k, n], (me, peer))
+
+    def stats_finish(k, values, gain_ref, bias_ref, out_ref):
+        tile = stats_out[k]
+        for n in range(tp_count - 1):
+            arrive(("stats", k, n), stats_in.at[k, n])
+            tile = tile + stats_in[k, n]
+        padded = jnp.concatenate(
+            [tile, jnp.zeros((rows - tile.shape[0], rows), f32)], axis=0
+        ).T
+        average = padded[:, 0:1] / full_width
+        spread = padded[:, 1:2] / full_width - average * average
+        scaled = (values - average) * lax.rsqrt(spread + 1e-05)
+        out_ref[...] = (
+            scaled * gain_ref[...].astype(f32) + bias_ref[...].astype(f32)
+        ).astype(bf16)
+
+    wait_routes(0)
+    arrive(("pair", 0), tokens.at[0, 1])
+    loads[2].wait()
+    loads[3].wait()
+    expert_up_stage(0)
+    for s in range(1, chips):
+        line_tokens(s)
+        if s == 1:
+            gather_relay(("shared",), shared_hidden)
+            gather_relay(("mixer",), weighted)
+    gather_relay(("tokens", 1), tokens.at[1, 0])
+    gather_relay(("hidden", 0), hidden.at[0])
+    for s in range(1, chips):
+        pair_tokens(s)
+        if s == 1:
+            gather_finish(("mixer",), weighted)
+            loads[4].wait()
+            mixed_ref[...] = dot(weighted[...], mix_v[...])
+            stats_start(0, mixed_ref[...])
+        if s + 1 < chips:
+            gather_relay(("tokens", s + 1), tokens.at[s + 1, 0])
+        wait_routes(s)
+        arrive(("pair", s), tokens.at[s, 1])
+        expert_up_stage(s)
+        if s == 1:
+            loads[5].wait()
+        gather_finish(("hidden", s - 1), hidden.at[s - 1])
+        expert_down_stage(s - 1)
+        gather_relay(("hidden", s), hidden.at[s])
+        expert_return(s - 1)
+    gather_finish(("shared",), shared_hidden)
+    loads[6].wait()
+    total_ref[...] = total_ref[...] + dot(shared_hidden[...], shared_down_v[...])
+    stats_finish(0, mixed_ref[...], gain_m_ref, bias_m_ref, out_m_ref)
+    last = chips - 1
+    gather_finish(("hidden", last), hidden.at[last])
+    expert_down_stage(last)
+    expert_return(last)
+    combined = total_ref[...]
+    for s in range(1, chips):
+        arrive(("return", s), returned.at[s])
+        combined = combined + returned[s].astype(f32)
+    stats_start(1, combined)
+    total_ref[...] = combined
+    stats_finish(1, total_ref[...], gain_e_ref, bias_e_ref, out_e_ref)
+    for item in started:
+        item.wait_send()
+
+
+def fused_device(
+    outer_gate,
+    inner_gate,
+    conv_value,
+    conv_taps,
+    mix_out,
+    gain_mixer,
+    bias_mixer,
+    moe_input,
+    route_ids,
+    route_weights,
+    expert_gate,
+    expert_up,
+    expert_down,
+    shared_gate,
+    shared_up,
+    shared_down,
+    gain_experts,
+    bias_experts,
+):
+    rows, cols = outer_gate.shape
+    width = moe_input.shape[1]
+    ep_count = lax.axis_size("ep")
+    tp_count = lax.axis_size("tp")
+    chips = ep_count // CORES
+    capacity = max(2, 3 * rows * route_ids.shape[1] // (2 * ep_count))
+    seq_length = rows * ep_count // SEQS
+    experts = jnp.arange(ep_count, dtype=jnp.int32)
+    named = route_ids.T[None, :, :] == experts[:, None, None]
+    dense = jnp.sum(jnp.where(named, route_weights.T[None, :, :], 0.0), axis=1)
+    bf16, f32 = jnp.bfloat16, jnp.float32
+    vmem = pl.BlockSpec(memory_space=pltpu.VMEM)
+    hbm = pl.BlockSpec(memory_space=pl.ANY)
+    copies = 16 * chips + 24
+    weight = pltpu.VMEM((width, cols), bf16)
+    scratch = [
+        *([weight] * 7),
+        pltpu.VMEM((chips, CORES, rows, width), bf16),
+        pltpu.VMEM((chips, CORES, ep_count, rows), f32),
+        pltpu.VMEM((CORES * capacity, width), bf16),
+        pltpu.VMEM((chips, CORES * capacity, width), bf16),
+        pltpu.VMEM((rows, width), bf16),
+        pltpu.VMEM((rows, width), bf16),
+        pltpu.VMEM((16, cols), bf16),
+        pltpu.VMEM((16, cols), bf16),
+        pltpu.VMEM((rows + 16, cols), f32),
+        pltpu.VMEM((chips, rows, cols), bf16),
+        pltpu.VMEM((chips, rows, cols), bf16),
+        pltpu.VMEM((chips, rows, cols), bf16),
+        pltpu.VMEM((chips, rows, cols), bf16),
+        pltpu.VMEM((2, 8, rows), f32),
+        pltpu.VMEM((2, tp_count - 1, 8, rows), f32),
+        pltpu.VMEM((rows, cols), f32),
+        pltpu.VMEM((rows, cols), f32),
+        pltpu.SemaphoreType.DMA((7,)),
+        pltpu.SemaphoreType.DMA((copies,)),
+        pltpu.SemaphoreType.DMA((copies,)),
+    ]
+    out = jax.ShapeDtypeStruct((rows, cols), bf16)
+    return pl.pallas_call(
+        functools.partial(fused_kernel, (ep_count, tp_count, capacity, seq_length)),
+        out_shape=(out, out),
+        in_specs=[vmem, vmem, vmem, vmem, hbm, vmem, vmem, vmem, vmem]
+        + [hbm] * 6
+        + [vmem, vmem],
+        out_specs=(vmem, vmem),
+        scratch_shapes=scratch,
+        compiler_params=pltpu.CompilerParams(
+            collective_id=0, has_side_effects=True, vmem_limit_bytes=VMEM_BYTES
+        ),
+    )(
+        outer_gate,
+        inner_gate,
+        conv_value,
+        conv_taps,
+        mix_out,
+        gain_mixer.reshape(1, cols),
+        bias_mixer.reshape(1, cols),
+        moe_input,
+        dense,
+        expert_gate,
+        expert_up,
+        expert_down,
+        shared_gate,
+        shared_up,
+        shared_down,
+        gain_experts.reshape(1, cols),
+        bias_experts.reshape(1, cols),
+    )
+
+
+def on_device(*arrays):
+    local_experts = arrays[10].shape[0]
+    square = lax.axis_size("tp") == PLANE * PLANE
+    if square and local_experts == 1 and lax.axis_size("ep") % CORES == 0:
+        return fused_device(*arrays)
+    return plain_device(*arrays)
+
+
 def solution(mesh):
     in_specs = (
         P("ep", "tp"),

time: 203 us -> 89.7 us (0.44)
  waiting for transfers between devices: 80.5 us -> 0 us
  Pallas kernels: 0 us -> 79.3 us
  blocking collectives: 57.7 us -> 0 us
  matrix products: 19.5 us -> 0 us
  between operations: 14.3 us -> 0.64 us
  other arithmetic: 10.6 us -> 1.3 us
  starting transfers between devices: 6.82 us -> 0 us
  local copies, waits for them, and re-layouts: 12.8 us -> 8.18 us
    all_gather x2 -> x0, waiting for transfers between devices: 80.5 us -> none  [the longest x1 42.8 us: on_device(): arrived = lax.all_gather(arrived, 'tp', axis=2, tiled=True)]
    pallas_call x0 -> x1, Pallas kernels: none -> 79.3 us  [fused_device(): pl.pallas_call(functools.partial(fused_kernel, (ep_count, tp_count, capac...]
    all_to_all x1 -> x0, blocking collectives: 27.2 us -> none  [on_device(): lax.all_to_all(sectioned, 'ep', split_axis=0, concat_axis=0, tiled=True)]
    all_gather x2 -> x0, blocking collectives: 21.6 us -> none  [the longest x1 11.2 us: on_device(): lax.all_gather(shared_hidden, 'tp', axis=1, tiled=True)]
    dot_general x7 -> x0, matrix products: 19.5 us -> none  [the longest x1 5.22 us: on_device(): jnp.einsum('secf,efd->secd', shaped, block, preferred_element_type=jnp.fl...]
    psum x1 -> x0, blocking collectives: 8.95 us -> none  [on_device(): lax.psum((jnp.sum(mixed, axis=1), jnp.sum(mixed * mixed, axis=1), jnp.sum...]
    convert_element_type x12 -> x0, other arithmetic: 7.3 us -> none  [the longest x2 2.07 us: finish(): offset_bias.astype(jnp.float32)]
    reshape x0 -> x4, local copies, waits for them, and re-layouts: none -> 5.05 us  [the longest x1 1.27 us: fused_device(): bias_experts.reshape(1, cols)]
  transfers between devices with their start and end apart: 4 -> 0, of which waited for: 2 -> 0; matrix products, arithmetic and copies ran while one was open for 9% -> 0% of each run, Pallas kernels for 0% -> 0%
where the time goes in v1:
time: 89.7 us; the launch traced here: 89.4 us
  Pallas kernels  79.3 us (88%)
  local copies, waits for them, and re-layouts  8.18 us (9%)
  other arithmetic  1.3 us (1%)
    pallas_call x1, Pallas kernels, fused_device(): pl.pallas_call(functools.partial(fused_kernel, (ep_count, tp_count, capac...  79.3 us
    unnamed x2, local copies, waits for them, and re-layouts  3.14 us

profile of v1, /device:TPU:0, one launch (start us, length us, event | category | flops | bytes accessed | tf_op | source)
XLA Modules:
  0.0 89.4 jit_solution(5812189388032707380)
XLA Ops:
  0.6 1.3 %reshape.18.gain_m_ref = bf16[1,512]{1,0:T(2,128)(2,1)} reshape(bf16[512]{0:T(512)(128)(2,1)} %param.23) | data formatting | bytes 2048 | tf_op jit(solution)/shard_map/reshape | solution.py:536
  1.9 1.3 %reshape.19.bias_m_ref = bf16[1,512]{1,0:T(2,128)(2,1)} reshape(bf16[512]{0:T(512)(128)(2,1)} %param.24) | data formatting | bytes 2048 | tf_op jit(solution)/shard_map/reshape | solution.py:537
  3.1 1.3 %reshape.20.gain_e_ref = bf16[1,512]{1,0:T(2,128)(2,1)} reshape(bf16[512]{0:T(512)(128)(2,1)} %param.34) | data formatting | bytes 2048 | tf_op jit(solution)/shard_map/reshape | solution.py:546
  4.4 1.3 %reshape.21.bias_e_ref = bf16[1,512]{1,0:T(2,128)(2,1)} reshape(bf16[512]{0:T(512)(128)(2,1)} %param.35) | data formatting | bytes 2048 | tf_op jit(solution)/shard_map/reshape | solution.py:547
  5.7 1.3 %select_reduce_fusion.weights_ref = f32[8,128]{1,0:T(8,128)} fusion(f32[4,128]{1,0:T(4,128)} %bitcast.2, s32[4,128]{1,0:T(4,128)} %bitcast.3), kind=kLoop, calls=%fused_computation | loop fusion | flops 11264 | bytes 8192 | tf_op jit(solution)/shard_map/reduce_sum | solution.py:489
  7.0 79.3 %shard_map.185 = (bf16[128,512]{1,0:T(8,128)(2,1)}, bf16[128,512]{1,0:T(8,128)(2,1)}) custom-call(bf16[128,512]{1,0:T(8,128)(2,1)} %outer_ref.1, bf16[128,512]{1,0:T(8,128)(2,1)} %inner_ref.1, bf16[128,512]{1,0:T(8,128)(2,1)} %value_ref.1, bf16[3,512]{1,0:T(4,128)(2,1)} %taps_ref.1, bf16[2048,512]{1,0:T(8,128)(2,1)} %mix_hbm.1, ...), custom_call_target="tpu_custom_call" | custom-call | tf_op jit(solution)/shard_map/pallas_call | solution.py:519
  86.3 1.6 %copy.22 = bf16[128,512]{1,0:T(8,128)(2,1)} copy(bf16[128,512]{1,0:T(8,128)(2,1)} %get-tuple-element.4) | data formatting | bytes 262144
  87.8 1.6 %copy.23 = bf16[128,512]{1,0:T(8,128)(2,1)} copy(bf16[128,512]{1,0:T(8,128)(2,1)} %get-tuple-element.5) | data formatting | bytes 262144

commit v2 on v1

--- a/solution.py
+++ b/solution.py
@@ -140,6 +140,37 @@
 VMEM_BYTES = 60 * 1024 * 1024
 
 
+def plan(chips):
+    steps = [("shared", 0), ("up", 0), ("hidden", 0)]
+    waiting = [("shared_relay", 0), ("mixer", 0)]
+    for s in range(1, chips):
+        steps.append(("line", s))
+        steps += waiting
+        waiting = [("token_relay", 1), ("hidden_relay", 0)] if s == 1 else []
+    steps += waiting + [("pair", 1)]
+    for s in range(1, chips):
+        if s + 1 < chips:
+            steps.append(("token_relay", s + 1))
+        if s == 1:
+            steps.append(("mixer_relay", 0))
+        if s == 2:
+            steps += [("mixer_dot", 0), ("hidden_relay", 1)]
+        if s > 1:
+            steps.append(("pair", s))
+        steps += [("up", s), ("hidden", s)]
+        if s > 2:
+            steps.append(("hidden_relay", s - 1))
+    steps.append(("shared_dot", 0))
+    for s in range(chips):
+        steps.append(("down", s))
+        if s == 0:
+            steps.append(("hidden_relay", chips - 1))
+        if s == chips - 2:
+            steps.append(("mixer_end", 0))
+        steps.append(("return", s))
+    return steps + [("collect", s) for s in range(1, chips)]
+
+
 def silu(value):
     return value / (1.0 + jnp.exp(-value))
 
@@ -154,7 +185,8 @@
     gain_m_ref,
     bias_m_ref,
     moe_ref,
-    weights_ref,
+    ids_ref,
+    route_w_ref,
     gate_hbm,
     up_hbm,
     down_hbm,
@@ -227,7 +259,11 @@
     edge[...] = product[rows - edge_rows :]
     pad = extended.shape[0] - rows
     extended[pad:, :] = product.astype(f32)
-    route[0, 0] = weights_ref[...]
+    named = lax.broadcasted_iota(jnp.int32, (ep_count, rows), 0)
+    dense = jnp.zeros((ep_count, rows), f32)
+    for k in range(ids_ref.shape[0]):
+        dense = dense + jnp.where(named == ids_ref[k : k + 1, :], route_w_ref[k : k + 1, :], 0.0)
+    route[0, 0] = dense
 
     barrier = pltpu.get_barrier_semaphore()
     for step in range(1, ep_count):
@@ -287,8 +323,8 @@
     for s in range(chips):
         target = (z - s + chips) % chips
         if s > 0:
-            send(("route", s, 0), weights_ref, route.at[s, 0], (target * CORES + c, j))
-        send(("route", s, 1), weights_ref, route.at[s, 1], (target * CORES + (1 - c), j))
+            send(("route", s, 0), route.at[0, 0], route.at[s, 0], (target * CORES + c, j))
+        send(("route", s, 1), route.at[0, 0], route.at[s, 1], (target * CORES + (1 - c), j))
     for s in range(1, chips):
         target = (z - s + chips) % chips
         send(
@@ -301,25 +337,6 @@
 
     def dot(a, b):
         return jnp.dot(a, b, preferred_element_type=f32)
-
-    loads[0].wait()
-    loads[1].wait()
-    held = silu(dot(moe_ref[...], shared_gate_v[...])) * dot(moe_ref[...], shared_up_v[...])
-    shared_hidden[:, columns(j)] = held.astype(bf16)
-    gather_start(("shared",), shared_hidden)
-
-    arrive(("edge",), border)
-    extended[pad - edge_rows : pad, :] = border[...].astype(f32)
-    places = (me * rows + lax.broadcasted_iota(jnp.int32, (rows, 1), 0)) % seq_length
-    taps_count = taps_ref.shape[0]
-    convolved = jnp.zeros((rows, cols), f32)
-    for offset in range(taps_count):
-        delay = taps_count - 1 - offset
-        delayed = extended[pad - delay : pad - delay + rows, :]
-        kept = (places >= delay).astype(f32)
-        convolved = convolved + taps_ref[offset : offset + 1, :].astype(f32) * delayed * kept
-    weighted[:, columns(j)] = (outer_ref[...].astype(f32) * convolved).astype(bf16)
-    gather_start(("mixer",), weighted)
 
     def token_ref(s, p):
         return moe_ref if (s, p) == (0, 0) else tokens.at[s, p]
@@ -343,7 +360,19 @@
             ).astype(bf16)
         held = silu(dot(rows_in[...], gate_v[...])) * dot(rows_in[...], up_v[...])
         hidden[s, :, columns(j)] = held.astype(bf16)
+
+    def hidden_start(s):
         gather_start(("hidden", s), hidden.at[s])
+
+    def hidden_relay(s):
+        gather_relay(("hidden", s), hidden.at[s])
+
+    def token_relay(s):
+        gather_relay(("tokens", s), tokens.at[s, 0])
+
+    def collect(s):
+        arrive(("return", s), returned.at[s])
+        total_ref[...] = total_ref[...] + returned[s].astype(f32)
 
     def expert_down_stage(s):
         full = dot(hidden[s], down_v[...])
@@ -358,7 +387,7 @@
                 own_part[s] = spread.astype(bf16)
                 send(("part", s), own_part.at[s], peer_part.at[s], (other, j))
             elif s == 0:
-                total_ref[...] = spread
+                total_ref[...] = total_ref[...] + spread
             else:
                 sent_sum[s] = spread.astype(bf16)
 
@@ -405,56 +434,93 @@
         spread = padded[:, 1:2] / full_width - average * average
         scaled = (values - average) * lax.rsqrt(spread + 1e-05)
         out_ref[...] = (
-            scaled * gain_ref[...].astype(f32) + bias_ref[...].astype(f32)
+            scaled * gain_ref[...].astype(f32).reshape(1, cols)
+            + bias_ref[...].astype(f32).reshape(1, cols)
         ).astype(bf16)
 
-    wait_routes(0)
-    arrive(("pair", 0), tokens.at[0, 1])
-    loads[2].wait()
-    loads[3].wait()
-    expert_up_stage(0)
-    for s in range(1, chips):
-        line_tokens(s)
-        if s == 1:
-            gather_relay(("shared",), shared_hidden)
-            gather_relay(("mixer",), weighted)
-    gather_relay(("tokens", 1), tokens.at[1, 0])
-    gather_relay(("hidden", 0), hidden.at[0])
-    for s in range(1, chips):
-        pair_tokens(s)
-        if s == 1:
-            gather_finish(("mixer",), weighted)
-            loads[4].wait()
-            mixed_ref[...] = dot(weighted[...], mix_v[...])
-            stats_start(0, mixed_ref[...])
-        if s + 1 < chips:
-            gather_relay(("tokens", s + 1), tokens.at[s + 1, 0])
+    def shared_start(_):
+        loads[0].wait()
+        loads[1].wait()
+        held = silu(dot(moe_ref[...], shared_gate_v[...])) * dot(moe_ref[...], shared_up_v[...])
+        shared_hidden[:, columns(j)] = held.astype(bf16)
+        gather_start(("shared",), shared_hidden)
+
+    def mixer_start(_):
+        arrive(("edge",), border)
+        extended[pad - edge_rows : pad, :] = border[...].astype(f32)
+        places = (me * rows + lax.broadcasted_iota(jnp.int32, (rows, 1), 0)) % seq_length
+        taps_count = taps_ref.shape[0]
+        convolved = jnp.zeros((rows, cols), f32)
+        for offset in range(taps_count):
+            delay = taps_count - 1 - offset
+            delayed = extended[pad - delay : pad - delay + rows, :]
+            kept = (places >= delay).astype(f32)
+            convolved = convolved + taps_ref[offset : offset + 1, :].astype(f32) * delayed * kept
+        weighted[:, columns(j)] = (outer_ref[...].astype(f32) * convolved).astype(bf16)
+        gather_start(("mixer",), weighted)
+
+    def expert_up_start(s):
         wait_routes(s)
         arrive(("pair", s), tokens.at[s, 1])
+        if s == 0:
+            loads[2].wait()
+            loads[3].wait()
         expert_up_stage(s)
-        if s == 1:
-            loads[5].wait()
-        gather_finish(("hidden", s - 1), hidden.at[s - 1])
-        expert_down_stage(s - 1)
-        gather_relay(("hidden", s), hidden.at[s])
-        expert_return(s - 1)
-    gather_finish(("shared",), shared_hidden)
-    loads[6].wait()
-    total_ref[...] = total_ref[...] + dot(shared_hidden[...], shared_down_v[...])
-    stats_finish(0, mixed_ref[...], gain_m_ref, bias_m_ref, out_m_ref)
-    last = chips - 1
-    gather_finish(("hidden", last), hidden.at[last])
-    expert_down_stage(last)
-    expert_return(last)
-    combined = total_ref[...]
-    for s in range(1, chips):
-        arrive(("return", s), returned.at[s])
-        combined = combined + returned[s].astype(f32)
-    stats_start(1, combined)
-    total_ref[...] = combined
+
+    def shared_relay(_):
+        gather_relay(("shared",), shared_hidden)
+
+    def mixer_relay(_):
+        gather_relay(("mixer",), weighted)
+
+    def mixer_dot(_):
+        gather_finish(("mixer",), weighted)
+        loads[4].wait()
+        mixed_ref[...] = dot(weighted[...], mix_v[...])
+        stats_start(0, mixed_ref[...])
+
+    def mixer_end(_):
+        stats_finish(0, mixed_ref[...], gain_m_ref, bias_m_ref, out_m_ref)
+
+    def shared_dot(_):
+        gather_finish(("shared",), shared_hidden)
+        loads[6].wait()
+        total_ref[...] = dot(shared_hidden[...], shared_down_v[...])
+        loads[5].wait()
+
+    def expert_down(s):
+        gather_finish(("hidden", s), hidden.at[s])
+        expert_down_stage(s)
+
+    acts = {
+        "shared": shared_start,
+        "mixer": mixer_start,
+        "shared_relay": shared_relay,
+        "mixer_relay": mixer_relay,
+        "mixer_dot": mixer_dot,
+        "mixer_end": mixer_end,
+        "shared_dot": shared_dot,
+        "line": line_tokens,
+        "token_relay": token_relay,
+        "pair": pair_tokens,
+        "up": expert_up_start,
+        "hidden": hidden_start,
+        "hidden_relay": hidden_relay,
+        "down": expert_down,
+        "return": expert_return,
+        "collect": collect,
+    }
+    for act, s in plan(chips):
+        acts[act](s)
+    stats_start(1, total_ref[...])
     stats_finish(1, total_ref[...], gain_e_ref, bias_e_ref, out_e_ref)
     for item in started:
         item.wait_send()
+
+
+def pass_kernel(first_ref, second_ref, out_first_ref, out_second_ref):
+    out_first_ref[...] = first_ref[...]
+    out_second_ref[...] = second_ref[...]
 
 
 def fused_device(
@@ -484,9 +550,6 @@
     chips = ep_count // CORES
     capacity = max(2, 3 * rows * route_ids.shape[1] // (2 * ep_count))
     seq_length = rows * ep_count // SEQS
-    experts = jnp.arange(ep_count, dtype=jnp.int32)
-    named = route_ids.T[None, :, :] == experts[:, None, None]
-    dense = jnp.sum(jnp.where(named, route_weights.T[None, :, :], 0.0), axis=1)
     bf16, f32 = jnp.bfloat16, jnp.float32
     vmem = pl.BlockSpec(memory_space=pltpu.VMEM)
     hbm = pl.BlockSpec(memory_space=pl.ANY)
@@ -516,10 +579,10 @@
         pltpu.SemaphoreType.DMA((copies,)),
     ]
     out = jax.ShapeDtypeStruct((rows, cols), bf16)
-    return pl.pallas_call(
+    first, second = pl.pallas_call(
         functools.partial(fused_kernel, (ep_count, tp_count, capacity, seq_length)),
         out_shape=(out, out),
-        in_specs=[vmem, vmem, vmem, vmem, hbm, vmem, vmem, vmem, vmem]
+        in_specs=[vmem] * 4 + [hbm] + [vmem] * 5
         + [hbm] * 6
         + [vmem, vmem],
         out_specs=(vmem, vmem),
@@ -533,19 +596,23 @@
         conv_value,
         conv_taps,
         mix_out,
-        gain_mixer.reshape(1, cols),
-        bias_mixer.reshape(1, cols),
+        gain_mixer,
+        bias_mixer,
         moe_input,
-        dense,
+        route_ids.T,
+        route_weights.T,
         expert_gate,
         expert_up,
         expert_down,
         shared_gate,
         shared_up,
         shared_down,
-        gain_experts.reshape(1, cols),
-        bias_experts.reshape(1, cols),
-    )
+        gain_experts,
+        bias_experts,
+    )
+    return pl.pallas_call(
+        pass_kernel, out_shape=(out, out), in_specs=[vmem, vmem], out_specs=(vmem, vmem)
+    )(first, second)
 
 
 def on_device(*arrays):

time: 89.7 us -> 76 us (0.85)
  local copies, waits for them, and re-layouts: 8.18 us -> 0 us
  Pallas kernels: 79.3 us -> 75 us
  other arithmetic: 1.3 us -> 0 us
    pallas_call x1, Pallas kernels: 79.3 us -> 73.3 us  [fused_device(): pl.pallas_call(functools.partial(fused_kernel, (ep_count, tp_count, capac...]
    reshape x4 -> x0, local copies, waits for them, and re-layouts: 5.05 us -> none  [the longest x1 1.27 us: fused_device(): bias_experts.reshape(1, cols)]
    unnamed x2 -> x0, local copies, waits for them, and re-layouts: 3.14 us -> none
    pallas_call x0 -> x1, Pallas kernels: none -> 1.68 us  [fused_device(): pl.pallas_call(pass_kernel, out_shape=(out, out), in_specs=[vmem, vmem],...]
    reduce_sum x1 -> x0, other arithmetic: 1.3 us -> none  [fused_device(): dense = jnp.sum(jnp.where(named, route_weights.T[None, :, :], 0.0), axis=1)]
where the time goes in v2:
time: 76 us; the launch traced here: 75.6 us
  Pallas kernels  75 us (99%)
    pallas_call x1, Pallas kernels, fused_device(): pl.pallas_call(functools.partial(fused_kernel, (ep_count, tp_count, capac...  73.3 us
    pallas_call x1, Pallas kernels, fused_device(): pl.pallas_call(pass_kernel, out_shape=(out, out), in_specs=[vmem, vmem],...  1.68 us

profile of v2, /device:TPU:0, one launch (start us, length us, event | category | flops | bytes accessed | tf_op | source)
XLA Modules:
  0.0 75.6 jit_solution(18310783879419959122)
XLA Ops:
  0.6 73.3 %shard_map.185 = (bf16[128,512]{1,0:T(8,128)(2,1)}, bf16[128,512]{1,0:T(8,128)(2,1)}) custom-call(bf16[128,512]{1,0:T(8,128)(2,1)} %outer_ref.1, bf16[128,512]{1,0:T(8,128)(2,1)} %inner_ref.1, bf16[128,512]{1,0:T(8,128)(2,1)} %value_ref.1, bf16[3,512]{1,0:T(4,128)(2,1)} %taps_ref.1, bf16[2048,512]{1,0:T(8,128)(2,1)} %mix_hbm.1, bf16[512]{0:T(512)(128)(2,1)} %gain_m_ref.1, ...), custom_call_target="tpu_custom_call" | custom-call | tf_op jit(solution)/shard_map/pallas_call | solution.py:582
  74.0 1.7 %shard_map.186 = (bf16[128,512]{1,0:T(8,128)(2,1)}, bf16[128,512]{1,0:T(8,128)(2,1)}) custom-call(bf16[128,512]{1,0:T(8,128)(2,1)} %get-tuple-element.4.first_ref, bf16[128,512]{1,0:T(8,128)(2,1)} %get-tuple-element.5.second_ref), custom_call_target="tpu_custom_call" | custom-call | tf_op jit(solution)/shard_map/pallas_call | solution.py:613
